TPU v7x, 32 devices: a whole 2x2x4 slice. The times are simulated.
32 devices in a mesh: sp: 8 (over z, x), tp: 4 (over y, core).
Axes of the slice: x: 2, y: 2, z: 4, core: 2. Of those that a mesh axis runs over, the one named last changes fastest.
Arguments:
- tokens: bfloat16 [2048, 4096], P(('sp', 'tp')), may hold values from -8 to 8, as said below
- q_weight: bfloat16 [4096, 4096], P('sp', 'tp'), may hold values from -0.09375 to 0.09375
- k_weight: bfloat16 [4096, 1024], P('sp', 'tp'), may hold values from -0.09375 to 0.09375
- v_weight: bfloat16 [4096, 1024], P('sp', 'tp'), may hold values from -0.09375 to 0.09375
- o_weight: bfloat16 [4096, 4096], P('tp', 'sp'), may hold values from -0.09375 to 0.09375
- q_gain: float32 [128], replicated, may hold values from 0.1 to 1.9
- k_gain: float32 [128], replicated, may hold values from 0.1 to 1.9
- out_gain: float32 [4096], replicated, may hold values from 0.1 to 1.9
Outputs:
- result: bfloat16 [2048, 4096], P(('sp', 'tp'))
Inputs may be any that keep to these rules, and one draw needn't show every extreme that they name: tokens are random draws plus a smooth per-channel wave along the sequence, so that their mean differs between parts of the sequence.
All inputs are finite; a program needn't handle non-finite values.
Results may differ from a plain program's by a relative error of at most 0.02.
Values may be sent and summed in bfloat16 or wider, within the bound.
A program may use at most 128 MiB of HBM per device.

v0:
```python
import jax
import jax.numpy as jnp
from jax import lax
from jax.sharding import PartitionSpec as P

GRID_W = 64


EPS = 1e-06
THETA = 10000.0


def tables(positions, head_dim):
    quarter = head_dim // 4
    grid_row = (positions // GRID_W).astype(jnp.float32)
    grid_col = (positions % GRID_W).astype(jnp.float32)
    inv_freq = 1.0 / THETA ** (jnp.arange(quarter, dtype=jnp.float32) * 2.0 / (head_dim // 2))
    ang_row = grid_row[:, None] * inv_freq[None, :]
    ang_col = grid_col[:, None] * inv_freq[None, :]
    angles = jnp.concatenate([ang_row, ang_row, ang_col, ang_col], axis=-1)
    return (jnp.cos(angles), jnp.sin(angles))


def norm_rope(raw_proj, gain_vec, positions):
    head_dim = raw_proj.shape[-1]
    values = raw_proj.astype(jnp.float32)
    values = values * lax.rsqrt(jnp.mean(values * values, axis=-1, keepdims=True) + EPS) * gain_vec
    cosine, sine_vals = tables(positions, head_dim)
    halves = values.reshape(values.shape[:-1] + (2, 2, head_dim // 4))
    rotated = jnp.stack([-halves[..., 1, :], halves[..., 0, :]], axis=-2).reshape(values.shape)
    return values * cosine[:, None, :] + rotated * sine_vals[:, None, :]


def on_device(tokens, q_weight, k_weight, v_weight, o_weight, q_gain, k_gain, out_gain):
    q_full, k_full, v_full, o_full = (
        lax.all_gather(q_weight, "sp", axis=0, tiled=True),
        lax.all_gather(k_weight, "sp", axis=0, tiled=True),
        lax.all_gather(v_weight, "sp", axis=0, tiled=True),
        lax.all_gather(o_weight, "sp", axis=1, tiled=True),
    )
    query_cols = q_full.shape[1]
    value_cols = k_full.shape[1]
    head_dim = q_gain.shape[0]
    local_kv = value_cols // head_dim
    groups = query_cols // value_cols

    def project(portion):
        return jnp.concatenate(
            [
                jnp.dot(portion, q_full, preferred_element_type=jnp.float32),
                jnp.dot(portion, k_full, preferred_element_type=jnp.float32),
                jnp.dot(portion, v_full, preferred_element_type=jnp.float32),
            ],
            axis=1,
        )

    projected = project(lax.all_gather(tokens, "tp", axis=0, tiled=True)).astype(jnp.bfloat16)
    tok_rows = projected.shape[0]
    positions = lax.axis_index("sp") * tok_rows + lax.iota(jnp.int32, tok_rows)
    queries = norm_rope(
        projected[:, :query_cols].reshape(tok_rows, local_kv * groups, head_dim), q_gain, positions
    )
    queries = queries.astype(jnp.bfloat16).reshape(tok_rows, local_kv, groups, head_dim)
    keys = norm_rope(
        projected[:, query_cols : query_cols + value_cols].reshape(tok_rows, local_kv, head_dim),
        k_gain,
        positions,
    )
    keys = keys.astype(jnp.bfloat16)
    values = projected[:, query_cols + value_cols :].reshape(tok_rows, local_kv, head_dim)
    score_scale = head_dim ** (-0.5)

    def absorb(state_in, key_blk, val_blk):
        run_max, run_sum, run_acc = state_in
        scores = (
            jnp.einsum("qkgd,tkd->kgqt", queries, key_blk, preferred_element_type=jnp.float32)
            * score_scale
        )
        new_max = jnp.maximum(run_max, jnp.max(scores, axis=-1))
        shrink = jnp.exp(run_max - new_max)
        probs_blk = jnp.exp(scores - new_max[..., None])
        run_sum = run_sum * shrink + jnp.sum(probs_blk, axis=-1)
        update = jnp.einsum(
            "kgqt,tkd->kgqd",
            probs_blk.astype(jnp.bfloat16),
            val_blk,
            preferred_element_type=jnp.float32,
        )
        run_acc = run_acc * shrink[..., None] + update
        return (new_max, run_sum, run_acc)

    def fold_keys(state_in, pieces):
        key_piece, val_piece = pieces
        row_count = key_piece.shape[0]
        width = 512 if row_count % 512 == 0 else row_count
        key_blocks = key_piece.reshape(row_count // width, width, local_kv, head_dim)
        val_blocks = val_piece.reshape(row_count // width, width, local_kv, head_dim)

        def scan_step(state_now, block_pair):
            return (absorb(state_now, block_pair[0], block_pair[1]), None)

        state_out, unused = lax.scan(scan_step, state_in, (key_blocks, val_blocks))
        return state_out

    initial = (
        jnp.full((local_kv, groups, tok_rows), -1e30, jnp.float32),
        jnp.zeros((local_kv, groups, tok_rows), jnp.float32),
        jnp.zeros((local_kv, groups, tok_rows, head_dim), jnp.float32),
    )
    run_max, run_sum, run_acc = fold_keys(
        initial,
        (
            lax.all_gather(keys, "sp", axis=0, tiled=True),
            lax.all_gather(values, "sp", axis=0, tiled=True),
        ),
    )
    attended = (
        (run_acc / run_sum[..., None])
        .transpose(2, 0, 1, 3)
        .reshape(tok_rows, query_cols)
        .astype(jnp.bfloat16)
    )

    def out_term():
        picked = lax.slice_in_dim(attended, 0, own_rows * lax.axis_size("tp"), axis=0)
        return jnp.dot(picked, o_full, preferred_element_type=jnp.float32)

    own_rows = tokens.shape[0]
    mixed = lax.psum_scatter(
        out_term().astype(jnp.bfloat16), "tp", scatter_dimension=0, tiled=True
    ).astype(jnp.float32)
    normed = mixed * lax.rsqrt(jnp.mean(mixed * mixed, axis=-1, keepdims=True) + EPS) * out_gain
    return normed.astype(jnp.bfloat16)


def solution(mesh):
    placed = (
        P(("sp", "tp"), None),
        P("sp", "tp"),
        P("sp", "tp"),
        P("sp", "tp"),
        P("tp", "sp"),
        P(),
        P(),
        P(),
    )
    return jax.shard_map(
        on_device, mesh=mesh, in_specs=placed, out_specs=P(("sp", "tp"), None), check_vma=False
    )
```

profile of v0, /device:TPU:0, one launch (start us, length us, event | category | flops | bytes accessed | tf_op | source)
XLA Modules:
  0.0 514.7 jit_solution(16533977301326256641)
XLA Ops:
  6.5 0.7 all-gather.8.cloned.1.call-update
  7.3 0.0 all-gather.10.cloned.1.call-start
  7.3 0.7 all-gather.10.cloned.1.call-update
  8.0 0.0 all-gather.16.cloned.1.call-start
  8.1 0.7 all-gather.16.cloned.1.call-update
  8.7 0.0 all-gather.12.cloned.1.call-start
  8.8 0.7 mul.208
  9.6 0.1 broadcast_multiply_fusion.1
  9.6 0.2 fusion.27
  9.9 24.3 %all-gather.8.cloned.1.call-done = bf16[256,4096]{1,0:T(8,128)(2,1)} async-done(((bf16[64,4096]{1,0:T(8,128)(2,1)}), bf16[256,4096]{1,0:T(8,128)(2,1)}) %all-gather.8.cloned.1.call-update) | async-done | bytes 2097168 | tf_op jit(solution)/shard_map/all_gather | solution.py:57
  34.2 51.4 %all-gather.10.cloned.1.call-done = bf16[4096,256]{1,0:T(8,128)(2,1)} async-done(((bf16[512,256]{1,0:T(8,128)(2,1)}), bf16[4096,256]{1,0:T(8,128)(2,1)}) %all-gather.10.cloned.1.call-update) | async-done | bytes 2097168 | tf_op jit(solution)/shard_map/all_gather | solution.py:37
  85.6 3.2 multiply_reduce_fusion
  88.8 0.1 multiply_multiply_fusion.1
  88.9 0.8 fusion.25
  89.7 0.0 all-gather.14.cloned.1.call-start
  89.8 0.5 all-gather.14.cloned.1.call-update
  90.3 0.0 all-gather.18.cloned.1.call-start
  90.4 45.5 %all-gather.16.cloned.1.call-done = bf16[4096,256]{1,0:T(8,128)(2,1)} async-done(((bf16[512,256]{1,0:T(8,128)(2,1)}), bf16[4096,256]{1,0:T(8,128)(2,1)}) %all-gather.16.cloned.1.call-update) | async-done | bytes 2097168 | tf_op jit(solution)/shard_map/all_gather | solution.py:38
  135.9 2.5 convolution_convert_fusion.2
  138.4 0.7 copy.63
  139.1 0.0 all-gather.18.cloned.1.call-update
  139.2 0.0 all-gather.20.cloned.1.call-start
  139.2 0.7 all-gather.20.cloned.1.call-update
  139.9 0.2 reduce-scatter.2.cloned.1.call-start
  140.2 0.7 mul.223
  140.8 35.3 %all-gather.12.cloned.1.call-done = bf16[2048,2,128]{0,2,1:T(8,128)(2,1)} async-done(((bf16[256,2,128]{0,2,1:T(8,128)(2,1)}), bf16[2048,2,128]{0,2,1:T(8,128)(2,1)}) %all-gather.12.cloned.1.call-update) | async-done | bytes 1048592 | tf_op jit(solution)/shard_map/all_gather | solution.py:113
  176.1 2.3 copy.59
  178.4 123.0 %all-gather.14.cloned.1.call-done = bf16[4096,1024]{1,0:T(8,128)(2,1)} async-done(((bf16[512,1024]{1,0:T(8,128)(2,1)}), bf16[4096,1024]{1,0:T(8,128)(2,1)}) %all-gather.14.cloned.1.call-update) | async-done | bytes 8388624 | tf_op jit(solution)/shard_map/all_gather | solution.py:36
  301.4 6.7 %fusion.19 = f32[256,1024]{1,0:T(8,128)} fusion(bf16[256,4096]{1,0:T(8,128)(2,1)S(1)} %copy-done.1, bf16[4096,1024]{1,0:T(8,128)(2,1)} %all-gather.14.cloned.1.call-done), kind=kOutput, calls=%fused_computation.26 | convolution fusion | flops 2148007936 | bytes 11534336 | tf_op jit(solution)/shard_map/dot_general | solution.py:50
  308.1 1.6 copy.71
  309.6 1.3 multiply_bitcast_fusion
  311.0 0.2 copy.74
  311.2 0.3 reduce_sum.37
  311.5 0.1 copy.60
  311.6 0.9 multiply_multiply_fusion
  312.5 0.1 slice_negate_fusion
  312.6 0.1 pad_maximum_fusion
  312.7 1.1 add_convert_fusion
  313.7 1.3 copy.65
  315.0 27.5 %all-gather.18.cloned.1.call-done = bf16[2048,2,128]{2,0,1:T(8,128)(2,1)} async-done(((bf16[256,2,128]{2,0,1:T(8,128)(2,1)}), bf16[2048,2,128]{2,0,1:T(8,128)(2,1)}) %all-gather.18.cloned.1.call-update) | async-done | bytes 1048592 | tf_op jit(solution)/shard_map/all_gather | solution.py:114
  342.5 37.7 %while.15 = (s32[]{:T(128)}, f32[2,4,256]{2,1,0:T(4,128)S(1)}, f32[2,4,256]{2,1,0:T(4,128)S(1)}, f32[2,4,256,128]{3,2,1,0:T(8,128)S(1)}, bf16[4,512,2,128]{3,1,0...) while((s32[]{:T(128)}, f32[2,4,256]{2,1,0:T(4,128)S(1)}, ...), condition=%wide.region_5.6_spmd.clone, body=%wide.region_2.5_spmd.clone.sunk | while | flops 546056192 | bytes 32638084 | solution.py:102
  342.5 3.6 bitcast_reduce_fusion.2
  346.2 3.0 fusion.49
  349.2 0.4 copy-done
  349.6 2.3 fusion.51
  352.0 3.6 bitcast_reduce_fusion.2
  355.6 3.0 fusion.49
  358.7 0.4 copy-done
  359.1 2.3 fusion.51
  361.4 3.6 bitcast_reduce_fusion.2
  365.1 3.0 fusion.49
  368.1 0.4 copy-done
  368.5 2.3 fusion.51
  370.9 3.6 bitcast_reduce_fusion.2
  374.5 3.0 fusion.49
  377.6 0.4 copy-done
  378.0 2.3 fusion.51
  380.3 0.3 copy.67
  380.6 0.1 divide_convert_fusion
  380.7 87.0 %all-gather.20.cloned.1.call-done = bf16[1024,4096]{1,0:T(8,128)(2,1)} async-done(((bf16[1024,512]{1,0:T(8,128)(2,1)}), bf16[1024,4096]{1,0:T(8,128)(2,1)}) %all-gather.20.cloned.1.call-update) | async-done | bytes 8388624 | tf_op jit(solution)/shard_map/all_gather | solution.py:39
  467.7 7.2 %convolution_convert_fusion = bf16[256,4096]{1,0:T(8,128)(2,1)} fusion(bf16[256,1024]{0,1:T(8,128)(2,1)S(1)} %bitcast.80, bf16[1024,4096]{1,0:T(8,128)(2,1)} %all-gather.20.cloned.1.call-done), kind=kOutput, calls=%fused_computation.22 | convolution fusion | flops 2148532224 | bytes 11010048 | tf_op jit(solution)/shard_map/dot_general | solution.py:126
  474.9 29.7 %reduce-scatter.2.cloned.1.call-done = bf16[64,4096]{1,0:T(8,128)(2,1)} async-done(((bf16[256,4096]{1,0:T(8,128)(2,1)}), bf16[64,4096]{1,0:T(8,128)(2,1)}) %reduce-scatter.2.cloned.1.call-update) | async-done | bytes 524304 | tf_op jit(solution)/shard_map/reduce_scatter | solution.py:129
  504.6 1.2 fusion.21
  505.8 2.0 fusion.23
  (40 shorter events, 0.3 us)
Async XLA Ops:
  6.5 82.4 %copy-start.3 = (f32[128]{0:T(128)S(1)}, f32[128]{0:T(128)}, u32[]{:S(2)}) copy-start(f32[128]{0:T(128)} %param.16) | copy-start | bytes 1540
  6.5 27.6 %all-gather.8.cloned.1.call-start = ((), (), s32[]{:S(2)}) async-start(), calls=%async_computation.1 | async-start | bytes 2621440 | tf_op jit(solution)/shard_map/all_gather | solution.py:57
  7.3 78.3 %all-gather.10.cloned.1.call-start = ((), (), s32[]{:S(2)}) async-start(), calls=%async_computation.2 | async-start | bytes 2359296 | tf_op jit(solution)/shard_map/all_gather | solution.py:37
  8.0 127.9 %all-gather.16.cloned.1.call-start = ((), (), s32[]{:S(2)}) async-start(), calls=%async_computation.5 | async-start | bytes 2359296 | tf_op jit(solution)/shard_map/all_gather | solution.py:38
  8.7 167.4 %all-gather.12.cloned.1.call-start = ((), (), s32[]{:S(2)}) async-start(), calls=%async_computation.3 | async-start | bytes 1179648 | tf_op jit(solution)/shard_map/all_gather | solution.py:113
  34.2 101.7 %copy-start.1 = (bf16[256,4096]{1,0:T(8,128)(2,1)S(1)}, bf16[256,4096]{1,0:T(8,128)(2,1)}, u32[]{:S(2)}) copy-start(bf16[256,4096]{1,0:T(8,128)(2,1)} %all-gather.8.cloned.1.call-done) | copy-start | bytes 6291460
  88.9 51.3 %copy-start.4 = (f32[128]{0:T(128)S(1)}, f32[128]{0:T(128)}, u32[]{:S(2)}) copy-start(f32[128]{0:T(128)} %param.15) | copy-start | bytes 1540
  89.7 211.7 %all-gather.14.cloned.1.call-start = ((), (), s32[]{:S(2)}) async-start(), calls=%async_computation.4 | async-start | bytes 9437184 | tf_op jit(solution)/shard_map/all_gather | solution.py:36
  90.3 252.2 %all-gather.18.cloned.1.call-start = ((), (), s32[]{:S(2)}) async-start(), calls=%async_computation.6 | async-start | bytes 1179648 | tf_op jit(solution)/shard_map/all_gather | solution.py:114
  139.2 328.5 %all-gather.20.cloned.1.call-start = ((), (), s32[]{:S(2)}) async-start(), calls=%async_computation.7 | async-start | bytes 9437184 | tf_op jit(solution)/shard_map/all_gather | solution.py:39
  139.9 364.6 %reduce-scatter.2.cloned.1.call-start = ((), (), s32[]{:S(2)}) async-start(), calls=%async_computation.8 | async-start | bytes 2621440 | tf_op jit(solution)/shard_map/reduce_scatter | solution.py:129
  311.6 1.1 copy-start.5
  346.2 3.4 copy-start
  355.6 3.4 copy-start
  365.1 3.4 copy-start
  374.5 3.4 copy-start
  467.7 38.1 %copy-start.2 = (f32[4096]{0:T(1024)S(1)}, f32[4096]{0:T(1024)}, u32[]{:S(2)}) copy-start(f32[4096]{0:T(1024)} %param.17) | copy-start | bytes 49156
Sparse Core Ops, SparseCore 0:
  8.9 25.2 all-gather.7
  36.3 49.2 all-gather.9
  87.7 48.1 all-gather.15
  137.8 38.3 all-gather.11
  178.1 123.2 all-gather.13
  303.4 39.0 all-gather.17
  344.6 123.0 all-gather.19
  475.0 29.4 reduce-scatter.1
where the time goes:
time: 515 us
  waiting for transfers between devices  427 us (83%)
  matrix products  43.4 us (8%)
  other arithmetic  20.6 us (4%)
  between operations  13.7 us (3%)
  local copies, waits for them, and re-layouts  9.42 us (2%)
    all_gather x1, waiting for transfers between devices, on_device(): lax.all_gather(q_weight, 'sp', axis=0, tiled=True)  123 us
    all_gather x1, waiting for transfers between devices, on_device(): lax.all_gather(o_weight, 'sp', axis=1, tiled=True)  87 us
    all_gather x1, waiting for transfers between devices, on_device(): lax.all_gather(k_weight, 'sp', axis=0, tiled=True)  51.4 us
    all_gather x1, waiting for transfers between devices, on_device(): lax.all_gather(v_weight, 'sp', axis=0, tiled=True)  45.5 us
    all_gather x1, waiting for transfers between devices, on_device(): lax.all_gather(keys, 'sp', axis=0, tiled=True)  35.3 us
    reduce_scatter x1, waiting for transfers between devices, on_device(): lax.psum_scatter(out_term().astype(jnp.bfloat16), 'tp', scatter_dimension...  29.7 us
    all_gather x1, waiting for transfers between devices, on_device(): lax.all_gather(values, 'sp', axis=0, tiled=True)  27.5 us
    all_gather x1, waiting for transfers between devices, on_device(): lax.all_gather(tokens, 'tp', axis=0, tiled=True)  24.3 us
  transfers between devices with their start and end apart: 8, of which 8 were waited for; matrix products, arithmetic and copies ran while one was open for 12% of the time, Pallas kernels for 0%

commit v1 on v0

--- a/solution.py
+++ b/solution.py
@@ -1,6 +1,10 @@
+import functools
+
 import jax
 import jax.numpy as jnp
 from jax import lax
+from jax.experimental import pallas as pl
+from jax.experimental.pallas import tpu as pltpu
 from jax.sharding import PartitionSpec as P
 
 GRID_W = 64
@@ -133,6 +137,353 @@
     return normed.astype(jnp.bfloat16)
 
 
+MESH = pl.DeviceIdType.MESH
+F32, BF16 = jnp.float32, jnp.bfloat16
+LOG2E = 1.4426950408889634
+
+
+def sem_shapes(Z, X, Y, C, J):
+    return {
+        "t1": (Z,),
+        "t2": (Y, Z),
+        "t3": (C, Y, Z),
+        "wkv": (X, 2),
+        "wq": (X, J),
+        "wo": (X,),
+        "pkv": (Z,),
+        "pq": (J, Z),
+        "kz": (Z,),
+        "kx": (X, Z),
+        "at": (J, Z),
+        "mc": (C, Z),
+        "my": (Y, Z),
+        "ft": (Z,),
+    }
+
+
+def fused_kernel(Z, X, Y, C, J, G, hd, names, *refs):
+    (tok, wq, wk, wv, wo, qg, kg, og, cos, sin, out) = refs[:11]
+    (T, WQX, WKX, WVX, WOX, PKV, RKV, AKV, PQ, RQ, AQ, KV, QB, AT, MB, MC, MS, MY, FS, FB) = refs[11:31]
+    sems = {n: (refs[31 + 2 * i], refs[32 + 2 * i]) for i, n in enumerate(names)}
+
+    sp, tp = lax.axis_index("sp"), lax.axis_index("tp")
+    z, x = lax.div(sp, X), lax.rem(sp, X)
+    y, c = lax.div(tp, C), lax.rem(tp, C)
+    R, D = tok.shape
+    TP = Y * C
+    TR = TP * R
+    Kx = wq.shape[0]
+    Kz = Kx * X
+    Gc = G * hd
+    Kc = J * hd
+    No = wo.shape[1]
+
+    def up(v, d, n):
+        return lax.rem(v + d, n)
+
+    def dn(v, d, n):
+        return lax.rem(v + n - d, n)
+
+    def dev(zz, xx, yy, cc):
+        return {"sp": zz * X + xx, "tp": yy * C + cc}
+
+    def zdev(d):
+        return dev(up(z, d, Z), x, y, c)
+
+    def xdev(d):
+        return dev(z, up(x, d, X), y, c)
+
+    def ydev(d):
+        return dev(z, x, up(y, d, Y), c)
+
+    def cdev(d):
+        return dev(z, x, y, up(c, d, C))
+
+    sent = []
+
+    def send(src, dst, name, idx, to):
+        s, r = sems[name]
+        cp = pltpu.make_async_remote_copy(
+            src_ref=src, dst_ref=dst, send_sem=s.at[idx], recv_sem=r.at[idx],
+            device_id=to, device_id_type=MESH,
+        )
+        cp.start()
+        sent.append(cp)
+
+    def recv(dst, name, idx):
+        s, r = sems[name]
+        pltpu.make_async_remote_copy(
+            src_ref=dst, dst_ref=dst, send_sem=s.at[idx], recv_sem=r.at[idx],
+            device_id=cdev(1), device_id_type=MESH,
+        ).wait_recv()
+
+    def cols(k, n):
+        return pl.ds(pl.multiple_of(k * n, n), n)
+
+    barrier = pltpu.get_barrier_semaphore()
+    peers = [zdev(d) for d in range(1, Z)] + [xdev(d) for d in range(1, X)]
+    peers += [ydev(d) for d in range(1, Y)] + [cdev(d) for d in range(1, C)]
+    for p in peers:
+        pl.semaphore_signal(barrier, inc=1, device_id=p, device_id_type=MESH)
+    pl.semaphore_wait(barrier, len(peers))
+
+    for d in range(1, Z):
+        send(tok.at[:, cols(up(z, d, Z), Kz)], T.at[z, tp], "t1", (d,), zdev(d))
+    for d in range(1, X):
+        send(wk, WKX.at[d - 1], "wkv", (d, 0), xdev(d))
+        send(wv, WVX.at[d - 1], "wkv", (d, 1), xdev(d))
+        for j in range(J):
+            send(wq.at[:, j * Gc : (j + 1) * Gc], WQX.at[d - 1, j], "wq", (d, j), xdev(d))
+    T[z, tp] = tok[:, cols(z, Kz)]
+    for d in range(Z):
+        zs = dn(z, d, Z)
+        src = T.at[zs, tp]
+        if d == 0:
+            src = tok.at[:, cols(z, Kz)]
+        else:
+            recv(src, "t1", (d,))
+        for e in range(1, Y):
+            send(src, T.at[zs, tp], "t2", (e, d), ydev(e))
+        for f in range(1, C):
+            send(src, T.at[zs, tp], "t3", (f, 0, d), cdev(f))
+    for d in range(Z):
+        zs = dn(z, d, Z)
+        for e in range(1, Y):
+            blk = T.at[zs, dn(y, e, Y) * C + c]
+            recv(blk, "t2", (e, d))
+            for f in range(1, C):
+                send(blk, blk, "t3", (f, e, d), cdev(f))
+    for d in range(Z):
+        for f in range(1, C):
+            for e in range(Y):
+                recv(T.at[dn(z, d, Z), dn(y, e, Y) * C + dn(c, f, C)], "t3", (f, e, d))
+
+    def tok_part(zp, xs):
+        return T[zp, :, :, cols(xs, Kx)].reshape(TR, Kx)
+
+    def dot(a, b):
+        return jnp.dot(a, b, preferred_element_type=F32)
+
+    def partial(zp, own, got):
+        acc = dot(tok_part(zp, x), own)
+        for d in range(1, X):
+            acc = acc + dot(tok_part(zp, dn(x, d, X)), got(d))
+        return acc
+
+    for d in range(1, X):
+        recv(WKX.at[d - 1], "wkv", (d, 0))
+        recv(WVX.at[d - 1], "wkv", (d, 1))
+    for d in list(range(1, Z)) + [0]:
+        zp = up(z, d, Z)
+        pk = partial(zp, wk[...], lambda q: WKX[q - 1])
+        pv = partial(zp, wv[...], lambda q: WVX[q - 1])
+        if d == 0:
+            AKV[:, :Kc] = pk
+            AKV[:, Kc:] = pv
+        else:
+            PKV[d - 1, :, :Kc] = pk.astype(BF16)
+            PKV[d - 1, :, Kc:] = pv.astype(BF16)
+            send(PKV.at[d - 1], RKV.at[d - 1], "pkv", (d,), zdev(d))
+
+    def query_partials(j):
+        for d in range(1, X):
+            recv(WQX.at[d - 1, j], "wq", (d, j))
+        for d in list(range(1, Z)) + [0]:
+            zp = up(z, d, Z)
+            pq = partial(zp, wq[:, j * Gc : (j + 1) * Gc], lambda q: WQX[q - 1, j])
+            if d == 0:
+                AQ[j] = pq
+            else:
+                PQ[j, d - 1] = pq.astype(BF16)
+                send(PQ.at[j, d - 1], RQ.at[j, d - 1], "pq", (j, d), zdev(d))
+
+    low = lax.rem(lax.broadcasted_iota(jnp.int32, (TR, hd), 1), hd // 2) < hd // 4
+
+    def turn(raw, gain):
+        v = raw.astype(BF16).astype(F32)
+        v = v * lax.rsqrt(jnp.mean(v * v, axis=-1, keepdims=True) + EPS) * gain
+        other = jnp.where(low, pltpu.roll(v, hd - hd // 4, 1), pltpu.roll(v, hd // 4, 1))
+        return (v * cos[...] + other * sin[...]).astype(BF16)
+
+    query_partials(0)
+
+    for d in range(1, Z):
+        recv(RKV.at[d - 1], "pkv", (d,))
+    kvsum = AKV[...]
+    for d in range(1, Z):
+        kvsum = kvsum + RKV[d - 1].astype(F32)
+    for j in range(J):
+        KV[sp, :, j * hd : (j + 1) * hd] = turn(kvsum[:, j * hd : (j + 1) * hd], kg[...])
+    KV[sp, :, Kc:] = kvsum[:, Kc:].astype(BF16)
+    for d in range(1, Z):
+        send(KV.at[sp], KV.at[sp], "kz", (d,), zdev(d))
+    for e in range(1, X):
+        send(KV.at[sp], KV.at[sp], "kx", (e, 0), xdev(e))
+
+    for j in range(1, J):
+        query_partials(j)
+    for d in range(1, X):
+        send(wo, WOX.at[d - 1], "wo", (d,), xdev(d))
+
+    for d in range(1, Z):
+        blk = KV.at[dn(z, d, Z) * X + x]
+        recv(blk, "kz", (d,))
+        for e in range(1, X):
+            send(blk, blk, "kx", (e, d), xdev(e))
+    for d in range(Z):
+        for e in range(1, X):
+            recv(KV.at[dn(z, d, Z) * X + dn(x, e, X)], "kx", (e, d))
+
+    scale = hd ** (-0.5) * LOG2E
+    for j in range(J):
+        for d in range(1, Z):
+            recv(RQ.at[j, d - 1], "pq", (j, d))
+
+        def one_head(g, carry):
+            here = cols(g, hd)
+            q = AQ[j, :, here]
+            for d in range(1, Z):
+                q = q + RQ[j, d - 1, :, here].astype(F32)
+            q = turn(q, qg[...])
+            keys = KV[:, :, j * hd : (j + 1) * hd].reshape(Z * X * TR, hd)
+            vals = KV[:, :, Kc + j * hd : Kc + (j + 1) * hd].reshape(Z * X * TR, hd)
+            s = lax.dot_general(q, keys, (((1,), (1,)), ((), ())), preferred_element_type=F32)
+            m = jnp.max(s, axis=-1, keepdims=True)
+            p = jnp.exp2((s - m) * scale)
+            total = jnp.sum(p, axis=-1, keepdims=True)
+            o = dot(p.astype(BF16), vals)
+            AT[z, j, :, here] = (o / total).astype(BF16)
+            return carry
+
+        lax.fori_loop(0, G, one_head, 0)
+        for d in range(1, Z):
+            send(AT.at[z, j], AT.at[z, j], "at", (j, d), zdev(d))
+
+    for d in range(1, X):
+        recv(WOX.at[d - 1], "wo", (d,))
+    for d in range(Z):
+        zp = dn(z, d, Z)
+        if d:
+            for j in range(J):
+                recv(AT.at[zp, j], "at", (j, d))
+        for e in range(X):
+            w = wo if e == 0 else WOX.at[e - 1]
+            acc = dot(AT[zp, 0], w[:Gc])
+            for j in range(1, J):
+                acc = acc + dot(AT[zp, j], w[j * Gc : (j + 1) * Gc])
+            MB[d, :, :, :, cols(dn(x, e, X), No)] = acc.astype(BF16).reshape(Y, C, R, No)
+        for f in range(1, C):
+            send(MB.at[d, :, up(c, f, C)], MC.at[f - 1, d], "mc", (f, d), cdev(f))
+    for d in range(Z):
+        total = MB[d, :, c].astype(F32)
+        for f in range(1, C):
+            recv(MC.at[f - 1, d], "mc", (f, d))
+            total = total + MC[f - 1, d].astype(F32)
+        MS[d] = total.astype(BF16)
+        for e in range(1, Y):
+            send(MS.at[d, up(y, e, Y)], MY.at[e - 1, d], "my", (e, d), ydev(e))
+    for d in list(range(1, Z)) + [0]:
+        total = MS[d, y].astype(F32)
+        for e in range(1, Y):
+            recv(MY.at[e - 1, d], "my", (e, d))
+            total = total + MY[e - 1, d].astype(F32)
+        if d == 0:
+            FB[z] = total.astype(BF16)
+        else:
+            FS[d - 1] = total.astype(BF16)
+            send(FS.at[d - 1], FB.at[z], "ft", (d,), dev(dn(z, d, Z), x, y, c))
+    for d in range(1, Z):
+        recv(FB.at[up(z, d, Z)], "ft", (d,))
+
+    square = jnp.zeros((R, 1), F32)
+    for k in range(Z):
+        v = FB[k].astype(F32)
+        square = square + jnp.sum(v * v, axis=-1, keepdims=True)
+    inv = lax.rsqrt(square * (1.0 / D) + EPS)
+    for k in range(Z):
+        part = slice(k * X * No, (k + 1) * X * No)
+        out[:, part] = (FB[k].astype(F32) * inv * og[:, part]).astype(BF16)
+    for cp in sent:
+        cp.wait_send()
+
+
+def split_axis(n):
+    return 2 if n % 2 == 0 else 1
+
+
+def fused_plan(n_sp, n_tp, tokens, q_weight, k_weight, o_weight, hd):
+    X, C = split_axis(n_sp), split_axis(n_tp)
+    Z, Y = n_sp // X, n_tp // C
+    R, D = tokens.shape
+    Kx, Qc = q_weight.shape
+    Kc = k_weight.shape[1]
+    J, G = Kc // hd, Qc // Kc
+    Gc, TR, No = G * hd, n_tp * R, o_weight.shape[1]
+    NX = X * No
+    V = pltpu.VMEM
+    scratch = [
+        ((Z, n_tp, R, Kx * X), BF16),
+        ((X - 1, J, Kx, Gc), BF16),
+        ((X - 1, Kx, Kc), BF16),
+        ((X - 1, Kx, Kc), BF16),
+        ((X - 1, Qc, No), BF16),
+        ((Z - 1, TR, 2 * Kc), BF16),
+        ((Z - 1, TR, 2 * Kc), BF16),
+        ((TR, 2 * Kc), F32),
+        ((J, Z - 1, TR, Gc), BF16),
+        ((J, Z - 1, TR, Gc), BF16),
+        ((J, TR, Gc), F32),
+        ((n_sp, TR, 2 * Kc), BF16),
+        ((G, 16, hd), BF16),
+        ((Z, J, TR, Gc), BF16),
+        ((Z, Y, C, R, NX), BF16),
+        ((C - 1, Z, Y, R, NX), BF16),
+        ((Z, Y, R, NX), BF16),
+        ((Y - 1, Z, R, NX), BF16),
+        ((Z - 1, R, NX), BF16),
+        ((Z, R, NX), BF16),
+    ]
+    size = 0
+    for shape, kind in scratch:
+        n = jnp.dtype(kind).itemsize
+        for k in shape:
+            n *= k
+        size += n
+    fits = min(Z, X, Y, C) > 1 and size + TR * n_sp * TR * 12 < 44 * 2**20
+    return fits, (Z, X, Y, C, J, G, hd), [V(s, k) for s, k in scratch]
+
+
+def fused_device(n_sp, n_tp, tokens, q_weight, k_weight, v_weight, o_weight, q_gain, k_gain, out_gain):
+    hd = q_gain.shape[0]
+    fits, dims, scratch = fused_plan(n_sp, n_tp, tokens, q_weight, k_weight, o_weight, hd)
+    if not fits:
+        return on_device(tokens, q_weight, k_weight, v_weight, o_weight, q_gain, k_gain, out_gain)
+    rows = n_tp * tokens.shape[0]
+    positions = lax.axis_index("sp") * rows + lax.iota(jnp.int32, rows)
+    cosine, sine = tables(positions, hd)
+    low = (jnp.arange(hd) % (hd // 2)) < hd // 4
+    sine = jnp.where(low[None, :], -sine, sine)
+    Z, X, Y, C, J = dims[:5]
+    shapes = sem_shapes(Z, X, Y, C, J)
+    names = list(shapes)
+    for n in names:
+        scratch += [pltpu.SemaphoreType.DMA(shapes[n]), pltpu.SemaphoreType.DMA(shapes[n])]
+    spec = pl.BlockSpec(memory_space=pltpu.VMEM)
+    return pl.pallas_call(
+        functools.partial(fused_kernel, *dims, names),
+        out_shape=jax.ShapeDtypeStruct(tokens.shape, BF16),
+        in_specs=[spec] * 10,
+        out_specs=spec,
+        scratch_shapes=scratch,
+        compiler_params=pltpu.CompilerParams(
+            collective_id=0, has_side_effects=True, vmem_limit_bytes=60 * 2**20
+        ),
+    )(
+        tokens, q_weight, k_weight, v_weight, o_weight,
+        q_gain[None, :], k_gain[None, :], out_gain[None, :], cosine, sine,
+    )
+
+
 def solution(mesh):
     placed = (
         P(("sp", "tp"), None),
@@ -145,5 +496,6 @@
         P(),
     )
     return jax.shard_map(
-        on_device, mesh=mesh, in_specs=placed, out_specs=P(("sp", "tp"), None), check_vma=False
-    )
+        functools.partial(fused_device, mesh.shape["sp"], mesh.shape["tp"]),
+        mesh=mesh, in_specs=placed, out_specs=P(("sp", "tp"), None), check_vma=False,
+    )

time: 515 us -> 193 us (0.37)
  waiting for transfers between devices: 427 us -> 0 us
  Pallas kernels: 0 us -> 190 us
  matrix products: 43.4 us -> 0 us
  other arithmetic: 20.6 us -> 1.43 us
  between operations: 13.7 us -> 0.02 us
  local copies, waits for them, and re-layouts: 9.42 us -> 1.87 us
    all_gather x7 -> x0, waiting for transfers between devices: 394 us -> none  [the longest x1 123 us: on_device(): lax.all_gather(q_weight, 'sp', axis=0, tiled=True)]
    pallas_call x0 -> x1, Pallas kernels: none -> 190 us  [fused_device(): pl.pallas_call(functools.partial(fused_kernel, *dims, names), out_shape=j...]
    dot_general x12 -> x0, matrix products: 43.4 us -> none  [the longest x4 14.5 us: absorb(): jnp.einsum('qkgd,tkd->kgqt', queries, key_blk, preferred_element_type=jnp...]
    reduce_scatter x1 -> x0, waiting for transfers between devices: 29.7 us -> none  [on_device(): lax.psum_scatter(out_term().astype(jnp.bfloat16), 'tp', scatter_dimension...]
    reduce_sum x6 -> x0, other arithmetic: 13.7 us -> none  [the longest x4 12.2 us: absorb(): run_sum = run_sum * shrink + jnp.sum(probs_blk, axis=-1)]
  transfers between devices with their start and end apart: 8 -> 0, of which waited for: 8 -> 0; matrix products, arithmetic and copies ran while one was open for 12% -> 0% of each run, Pallas kernels for 0% -> 0%
where the time goes in v1:
time: 193 us
  Pallas kernels  190 us (98%)
    pallas_call x1, Pallas kernels, fused_device(): pl.pallas_call(functools.partial(fused_kernel, *dims, names), out_shape=j...  190 us

profile of v1, /device:TPU:0, one launch (start us, length us, event | category | flops | bytes accessed | tf_op | source)
XLA Modules:
  0.0 193.0 jit_solution(4574706334780981461)
XLA Ops:
  0.0 0.1 broadcast_multiply_fusion.1
  0.2 1.3 negate_select_fusion
  1.4 189.7 %shard_map.82 = bf16[64,4096]{1,0:T(8,128)(2,1)} custom-call(bf16[64,4096]{1,0:T(8,128)(2,1)} %refs_0_.1, bf16[512,1024]{1,0:T(8,128)(2,1)} %refs_1_.1, bf16[512,256]{1,0:T(8,128)(2,1)} %refs_2_.1, bf16[512,256]{1,0:T(8,128)(2,1)} %refs_3_.1, bf16[1024,512]{1,0:T(8,128)(2,1)} %refs_4_.1, f32[1,128]{1,0:T(1,128)} %bitcast.4, f32[1,128]{1,0:T(1,128)} %bitcast.5, ...), custom_call_target="tpu_custom_call" | custom-call | tf_op jit(solution)/shard_map/pallas_call | solution.py:472
  191.2 1.9 copy.10
  (3 shorter events, 0.0 us)

commit v2 on v1

--- a/solution.py
+++ b/solution.py
@@ -150,11 +150,11 @@
         "wkv": (X, 2),
         "wq": (X, J),
         "wo": (X,),
-        "pkv": (Z,),
-        "pq": (J, Z),
-        "kz": (Z,),
+        "pkv": (Z + 1,),
+        "pq": (J, Z + 1),
+        "kz": (Z + 1,),
         "kx": (X, Z),
-        "at": (J, Z),
+        "at": (J, Z + 1),
         "mc": (C, Z),
         "my": (Y, Z),
         "ft": (Z,),
@@ -163,8 +163,8 @@
 
 def fused_kernel(Z, X, Y, C, J, G, hd, names, *refs):
     (tok, wq, wk, wv, wo, qg, kg, og, cos, sin, out) = refs[:11]
-    (T, WQX, WKX, WVX, WOX, PKV, RKV, AKV, PQ, RQ, AQ, KV, QB, AT, MB, MC, MS, MY, FS, FB) = refs[11:31]
-    sems = {n: (refs[31 + 2 * i], refs[32 + 2 * i]) for i, n in enumerate(names)}
+    (T, WQX, WKX, WVX, WOX, PKV, RKV, AKV, PQ, RQ, AQ, KV, AT, MB, MC, MS, MY, FS, FB) = refs[11:30]
+    sems = {n: (refs[30 + 2 * i], refs[31 + 2 * i]) for i, n in enumerate(names)}
 
     sp, tp = lax.axis_index("sp"), lax.axis_index("tp")
     z, x = lax.div(sp, X), lax.rem(sp, X)
@@ -201,14 +201,21 @@
 
     sent = []
 
-    def send(src, dst, name, idx, to):
+    def send(src, dst, name, idx, to, ridx=None, when=None):
         s, r = sems[name]
-        cp = pltpu.make_async_remote_copy(
-            src_ref=src, dst_ref=dst, send_sem=s.at[idx], recv_sem=r.at[idx],
-            device_id=to, device_id_type=MESH,
-        )
-        cp.start()
-        sent.append(cp)
+        ridx = idx if ridx is None else ridx
+
+        def make():
+            return pltpu.make_async_remote_copy(
+                src_ref=src, dst_ref=dst, send_sem=s.at[idx], recv_sem=r.at[ridx],
+                device_id=to, device_id_type=MESH,
+            )
+
+        if when is None:
+            make().start()
+        else:
+            pl.when(when)(lambda: make().start())
+        sent.append((make, when))
 
     def recv(dst, name, idx):
         s, r = sems[name]
@@ -219,6 +226,27 @@
 
     def cols(k, n):
         return pl.ds(pl.multiple_of(k * n, n), n)
+
+    def pick(rows_by_z, n):
+        v = 0
+        for k in range(Z):
+            v = v + jnp.where(z == k, rows_by_z[k][n], 0)
+        return v
+
+    near = [sorted([k for k in range(Z) if k != q], key=lambda k: abs(k - q)) for q in range(Z)]
+    far = [sorted(r, key=lambda k: -abs(k - q)) for q, r in enumerate(near)]
+    above, below = z < Z - 1, z > 0
+
+    def line_own(ref, at, name, pre):
+        send(ref.at[at], ref.at[at], name, pre + (z,), dev(z + 1, x, y, c), when=above)
+        send(ref.at[at], ref.at[at], name, pre + (Z,), dev(z - 1, x, y, c), ridx=pre + (z,), when=below)
+
+    def line_hop(zp, ref, at, name, pre):
+        recv(ref.at[at], name, pre + (zp,))
+        go_up = jnp.logical_and(zp < z, above)
+        go_down = jnp.logical_and(zp > z, below)
+        step = jnp.where(zp < z, 1, -1)
+        send(ref.at[at], ref.at[at], name, pre + (zp,), dev(z + step, x, y, c), when=jnp.logical_or(go_up, go_down))
 
     barrier = pltpu.get_barrier_semaphore()
     peers = [zdev(d) for d in range(1, Z)] + [xdev(d) for d in range(1, X)]
@@ -270,32 +298,59 @@
             acc = acc + dot(tok_part(zp, dn(x, d, X)), got(d))
         return acc
 
+    def line_sum(n, acc_of, pre, Ps, Rs, name):
+        zp = pick(far, n)
+        acc = acc_of(zp)
+        relay = jnp.where(zp > z, z, Z - 1 - z) > 0
+
+        @pl.when(relay)
+        def _():
+            recv(Rs(zp), name, pre + (zp,))
+            Ps(n)[...] = (acc + Rs(zp)[...].astype(F32)).astype(BF16)
+
+        @pl.when(jnp.logical_not(relay))
+        def _():
+            Ps(n)[...] = acc.astype(BF16)
+
+        step = jnp.where(zp > z, 1, -1)
+        slot = jnp.where(zp == z - 1, Z, zp)
+        send(Ps(n), Rs(slot), name, pre + (n,), dev(z + step, x, y, c), ridx=pre + (slot,))
+
+    def line_total(A, pre, Rs, name):
+        for cond, slot in ((below, z), (above, Z)):
+
+            @pl.when(cond)
+            def _():
+                recv(Rs(slot), name, pre + (slot,))
+                A[...] = A[...] + Rs(slot)[...].astype(F32)
+
+    def kv_partial(zp):
+        pk = partial(zp, wk[...], lambda q: WKX[q - 1])
+        pv = partial(zp, wv[...], lambda q: WVX[q - 1])
+        return jnp.concatenate([pk, pv], axis=1)
+
+    def kv_step(n):
+        line_sum(n, kv_partial, (), lambda k: PKV.at[k], lambda k: RKV.at[k], "pkv")
+
+    def q_partial(j):
+        return lambda zp: partial(zp, wq[:, j * Gc : (j + 1) * Gc], lambda q: WQX[q - 1, j])
+
+    def q_step(j, n):
+        if n == 0:
+            for d in range(1, X):
+                recv(WQX.at[d - 1, j], "wq", (d, j))
+        line_sum(n, q_partial(j), (j,), lambda k: PQ.at[j, k], lambda k: RQ.at[j, k], "pq")
+        if n == Z - 2:
+            AQ[j] = q_partial(j)(z)
+
     for d in range(1, X):
         recv(WKX.at[d - 1], "wkv", (d, 0))
         recv(WVX.at[d - 1], "wkv", (d, 1))
-    for d in list(range(1, Z)) + [0]:
-        zp = up(z, d, Z)
-        pk = partial(zp, wk[...], lambda q: WKX[q - 1])
-        pv = partial(zp, wv[...], lambda q: WVX[q - 1])
-        if d == 0:
-            AKV[:, :Kc] = pk
-            AKV[:, Kc:] = pv
-        else:
-            PKV[d - 1, :, :Kc] = pk.astype(BF16)
-            PKV[d - 1, :, Kc:] = pv.astype(BF16)
-            send(PKV.at[d - 1], RKV.at[d - 1], "pkv", (d,), zdev(d))
-
-    def query_partials(j):
-        for d in range(1, X):
-            recv(WQX.at[d - 1, j], "wq", (d, j))
-        for d in list(range(1, Z)) + [0]:
-            zp = up(z, d, Z)
-            pq = partial(zp, wq[:, j * Gc : (j + 1) * Gc], lambda q: WQX[q - 1, j])
-            if d == 0:
-                AQ[j] = pq
-            else:
-                PQ[j, d - 1] = pq.astype(BF16)
-                send(PQ.at[j, d - 1], RQ.at[j, d - 1], "pq", (j, d), zdev(d))
+    for n in range(Z - 1):
+        kv_step(n)
+    AKV[...] = kv_partial(z)
+    q_steps = [(j, n) for j in range(J) for n in range(Z - 1)]
+    q_step(*q_steps.pop(0))
 
     low = lax.rem(lax.broadcasted_iota(jnp.int32, (TR, hd), 1), hd // 2) < hd // 4
 
@@ -305,46 +360,39 @@
         other = jnp.where(low, pltpu.roll(v, hd - hd // 4, 1), pltpu.roll(v, hd // 4, 1))
         return (v * cos[...] + other * sin[...]).astype(BF16)
 
-    query_partials(0)
-
-    for d in range(1, Z):
-        recv(RKV.at[d - 1], "pkv", (d,))
-    kvsum = AKV[...]
-    for d in range(1, Z):
-        kvsum = kvsum + RKV[d - 1].astype(F32)
+    line_total(AKV, (), lambda k: RKV.at[k], "pkv")
     for j in range(J):
-        KV[sp, :, j * hd : (j + 1) * hd] = turn(kvsum[:, j * hd : (j + 1) * hd], kg[...])
-    KV[sp, :, Kc:] = kvsum[:, Kc:].astype(BF16)
-    for d in range(1, Z):
-        send(KV.at[sp], KV.at[sp], "kz", (d,), zdev(d))
+        KV[sp, :, j * hd : (j + 1) * hd] = turn(AKV[:, j * hd : (j + 1) * hd], kg[...])
+    KV[sp, :, Kc:] = AKV[:, Kc:].astype(BF16)
+    line_own(KV, sp, "kz", ())
     for e in range(1, X):
-        send(KV.at[sp], KV.at[sp], "kx", (e, 0), xdev(e))
-
-    for j in range(1, J):
-        query_partials(j)
+        send(KV.at[sp], KV.at[sp], "kx", (e, z), xdev(e))
+
+    def kv_hop(n):
+        zp = pick(near, n)
+        line_hop(zp, KV, zp * X + x, "kz", ())
+        for e in range(1, X):
+            send(KV.at[zp * X + x], KV.at[zp * X + x], "kx", (e, zp), xdev(e))
+
+    for n in range(Z - 1):
+        if q_steps:
+            q_step(*q_steps.pop(0))
+        kv_hop(n)
+    for step in q_steps:
+        q_step(*step)
     for d in range(1, X):
         send(wo, WOX.at[d - 1], "wo", (d,), xdev(d))
-
-    for d in range(1, Z):
-        blk = KV.at[dn(z, d, Z) * X + x]
-        recv(blk, "kz", (d,))
+    for k in range(Z):
         for e in range(1, X):
-            send(blk, blk, "kx", (e, d), xdev(e))
-    for d in range(Z):
-        for e in range(1, X):
-            recv(KV.at[dn(z, d, Z) * X + dn(x, e, X)], "kx", (e, d))
+            recv(KV.at[k * X + dn(x, e, X)], "kx", (e, k))
 
     scale = hd ** (-0.5) * LOG2E
     for j in range(J):
-        for d in range(1, Z):
-            recv(RQ.at[j, d - 1], "pq", (j, d))
+        line_total(AQ.at[j], (j,), lambda k: RQ.at[j, k], "pq")
 
         def one_head(g, carry):
             here = cols(g, hd)
-            q = AQ[j, :, here]
-            for d in range(1, Z):
-                q = q + RQ[j, d - 1, :, here].astype(F32)
-            q = turn(q, qg[...])
+            q = turn(AQ[j, :, here], qg[...])
             keys = KV[:, :, j * hd : (j + 1) * hd].reshape(Z * X * TR, hd)
             vals = KV[:, :, Kc + j * hd : Kc + (j + 1) * hd].reshape(Z * X * TR, hd)
             s = lax.dot_general(q, keys, (((1,), (1,)), ((), ())), preferred_element_type=F32)
@@ -356,44 +404,60 @@
             return carry
 
         lax.fori_loop(0, G, one_head, 0)
-        for d in range(1, Z):
-            send(AT.at[z, j], AT.at[z, j], "at", (j, d), zdev(d))
+        for up_down in ((z, z + 1, above), (Z, z - 1, below)):
+            send(AT.at[z, j], AT.at[z, j], "at", (j, up_down[0]), dev(up_down[1], x, y, c), ridx=(j, z), when=up_down[2])
 
     for d in range(1, X):
         recv(WOX.at[d - 1], "wo", (d,))
-    for d in range(Z):
-        zp = dn(z, d, Z)
-        if d:
-            for j in range(J):
-                recv(AT.at[zp, j], "at", (j, d))
+
+    def out_block(zp):
         for e in range(X):
             w = wo if e == 0 else WOX.at[e - 1]
             acc = dot(AT[zp, 0], w[:Gc])
             for j in range(1, J):
                 acc = acc + dot(AT[zp, j], w[j * Gc : (j + 1) * Gc])
-            MB[d, :, :, :, cols(dn(x, e, X), No)] = acc.astype(BF16).reshape(Y, C, R, No)
+            MB[zp, :, :, :, cols(dn(x, e, X), No)] = acc.astype(BF16).reshape(Y, C, R, No)
         for f in range(1, C):
-            send(MB.at[d, :, up(c, f, C)], MC.at[f - 1, d], "mc", (f, d), cdev(f))
-    for d in range(Z):
-        total = MB[d, :, c].astype(F32)
+            send(MB.at[zp, :, up(c, f, C)], MC.at[f - 1, zp], "mc", (f, zp), cdev(f))
+
+    def core_block(zp):
+        total = MB[zp, :, c].astype(F32)
         for f in range(1, C):
-            recv(MC.at[f - 1, d], "mc", (f, d))
-            total = total + MC[f - 1, d].astype(F32)
-        MS[d] = total.astype(BF16)
+            recv(MC.at[f - 1, zp], "mc", (f, zp))
+            total = total + MC[f - 1, zp].astype(F32)
+        MS[zp] = total.astype(BF16)
         for e in range(1, Y):
-            send(MS.at[d, up(y, e, Y)], MY.at[e - 1, d], "my", (e, d), ydev(e))
-    for d in list(range(1, Z)) + [0]:
-        total = MS[d, y].astype(F32)
+            send(MS.at[zp, up(y, e, Y)], MY.at[e - 1, zp], "my", (e, zp), ydev(e))
+
+    def row_block(zp, n):
+        total = MS[zp, y].astype(F32)
         for e in range(1, Y):
-            recv(MY.at[e - 1, d], "my", (e, d))
-            total = total + MY[e - 1, d].astype(F32)
-        if d == 0:
+            recv(MY.at[e - 1, zp], "my", (e, zp))
+            total = total + MY[e - 1, zp].astype(F32)
+        if n == 0:
             FB[z] = total.astype(BF16)
         else:
-            FS[d - 1] = total.astype(BF16)
-            send(FS.at[d - 1], FB.at[z], "ft", (d,), dev(dn(z, d, Z), x, y, c))
-    for d in range(1, Z):
-        recv(FB.at[up(z, d, Z)], "ft", (d,))
+            FS[n - 1] = total.astype(BF16)
+            send(FS.at[n - 1], FB.at[z], "ft", (n,), dev(zp, x, y, c), ridx=(z,))
+
+    blocks = [z] + [pick(near, n) for n in range(Z - 1)]
+    for n in range(Z + 2):
+        if n < Z:
+            zp = blocks[n]
+            if n:
+                for j in range(J):
+                    blk = AT.at[zp, j]
+                    recv(blk, "at", (j, zp))
+                    onward = jnp.where(zp < z, Z - 1 - z, z) > 0
+                    step = jnp.where(zp < z, 1, -1)
+                    send(blk, blk, "at", (j, zp), dev(z + step, x, y, c), when=onward)
+            out_block(zp)
+        if 1 <= n <= Z:
+            core_block(blocks[n - 1])
+        if n >= 2:
+            row_block(blocks[n - 2], n - 2)
+    for n in range(1, Z):
+        recv(FB.at[blocks[n]], "ft", (blocks[n],))
 
     square = jnp.zeros((R, 1), F32)
     for k in range(Z):
@@ -403,8 +467,11 @@
     for k in range(Z):
         part = slice(k * X * No, (k + 1) * X * No)
         out[:, part] = (FB[k].astype(F32) * inv * og[:, part]).astype(BF16)
-    for cp in sent:
-        cp.wait_send()
+    for make, when in sent:
+        if when is None:
+            make().wait_send()
+        else:
+            pl.when(when)(lambda make=make: make().wait_send())
 
 
 def split_axis(n):
@@ -428,13 +495,12 @@
         ((X - 1, Kx, Kc), BF16),
         ((X - 1, Qc, No), BF16),
         ((Z - 1, TR, 2 * Kc), BF16),
-        ((Z - 1, TR, 2 * Kc), BF16),
+        ((Z + 1, TR, 2 * Kc), BF16),
         ((TR, 2 * Kc), F32),
         ((J, Z - 1, TR, Gc), BF16),
-        ((J, Z - 1, TR, Gc), BF16),
+        ((J, Z + 1, TR, Gc), BF16),
         ((J, TR, Gc), F32),
         ((n_sp, TR, 2 * Kc), BF16),
-        ((G, 16, hd), BF16),
         ((Z, J, TR, Gc), BF16),
         ((Z, Y, C, R, NX), BF16),
         ((C - 1, Z, Y, R, NX), BF16),

time: 193 us -> 166 us (0.86)
  Pallas kernels: 190 us -> 162 us
    pallas_call x1, Pallas kernels: 190 us -> 162 us  [fused_device(): pl.pallas_call(functools.partial(fused_kernel, *dims, names), out_shape=j...]
where the time goes in v2:
time: 166 us
  Pallas kernels  162 us (98%)
  local copies, waits for them, and re-layouts  1.87 us (1%)
    pallas_call x1, Pallas kernels, fused_device(): pl.pallas_call(functools.partial(fused_kernel, *dims, names), out_shape=j...  162 us

profile of v2, /device:TPU:0, one launch (start us, length us, event | category | flops | bytes accessed | tf_op | source)
XLA Modules:
  0.0 165.5 jit_solution(5888661489953546476)
XLA Ops:
  0.0 0.1 broadcast_multiply_fusion.1
  0.2 1.3 negate_select_fusion
  1.4 162.2 %shard_map.82 = bf16[64,4096]{1,0:T(8,128)(2,1)} custom-call(bf16[64,4096]{1,0:T(8,128)(2,1)} %refs_0_.1, bf16[512,1024]{1,0:T(8,128)(2,1)} %refs_1_.1, bf16[512,256]{1,0:T(8,128)(2,1)} %refs_2_.1, bf16[512,256]{1,0:T(8,128)(2,1)} %refs_3_.1, bf16[1024,512]{1,0:T(8,128)(2,1)} %refs_4_.1, f32[1,128]{1,0:T(1,128)} %bitcast.4, f32[1,128]{1,0:T(1,128)} %bitcast.5, ...), custom_call_target="tpu_custom_call" | custom-call | tf_op jit(solution)/shard_map/pallas_call | solution.py:538
  163.6 1.9 %copy.10 = bf16[64,4096]{1,0:T(8,128)(2,1)} copy(bf16[64,4096]{1,0:T(8,128)(2,1)} %shard_map.82) | data formatting | bytes 1048576
  (3 shorter events, 0.0 us)

commit v3 on v2

--- a/solution.py
+++ b/solution.py
@@ -140,6 +140,7 @@
 MESH = pl.DeviceIdType.MESH
 F32, BF16 = jnp.float32, jnp.bfloat16
 LOG2E = 1.4426950408889634
+H = 2
 
 
 def sem_shapes(Z, X, Y, C, J):
@@ -149,9 +150,9 @@
         "t3": (C, Y, Z),
         "wkv": (X, 2),
         "wq": (X, J),
-        "wo": (X,),
-        "pkv": (Z + 1,),
-        "pq": (J, Z + 1),
+        "wo": (X, J),
+        "pkv": (Z + 1, H),
+        "pq": (J, Z + 1, H),
         "kz": (Z + 1,),
         "kx": (X, Z),
         "at": (J, Z + 1),
@@ -201,7 +202,13 @@
 
     sent = []
 
-    def send(src, dst, name, idx, to, ridx=None, when=None):
+    def wait_for(src, name, idx):
+        return lambda: pltpu.make_async_remote_copy(
+            src_ref=src, dst_ref=src, send_sem=sems[name][0].at[idx], recv_sem=sems[name][1].at[idx],
+            device_id=cdev(1), device_id_type=MESH,
+        ).wait_send()
+
+    def send(src, dst, name, idx, to, ridx=None, when=None, keep=True):
         s, r = sems[name]
         ridx = idx if ridx is None else ridx
 
@@ -215,7 +222,8 @@
             make().start()
         else:
             pl.when(when)(lambda: make().start())
-        sent.append((make, when))
+        if keep:
+            sent.append((wait_for(src, name, idx), when))
 
     def recv(dst, name, idx):
         s, r = sems[name]
@@ -303,25 +311,34 @@
         acc = acc_of(zp)
         relay = jnp.where(zp > z, z, Z - 1 - z) > 0
 
-        @pl.when(relay)
-        def _():
-            recv(Rs(zp), name, pre + (zp,))
-            Ps(n)[...] = (acc + Rs(zp)[...].astype(F32)).astype(BF16)
-
-        @pl.when(jnp.logical_not(relay))
-        def _():
-            Ps(n)[...] = acc.astype(BF16)
-
         step = jnp.where(zp > z, 1, -1)
         slot = jnp.where(zp == z - 1, Z, zp)
-        send(Ps(n), Rs(slot), name, pre + (n,), dev(z + step, x, y, c), ridx=pre + (slot,))
+        for h in range(H):
+            rows = slice(h * TR // H, (h + 1) * TR // H)
+            part = acc[rows]
+
+            @pl.when(relay)
+            def _():
+                got = Rs(zp).at[rows]
+                recv(got, name, pre + (zp, h))
+                Ps(n)[rows] = (part + got[...].astype(F32)).astype(BF16)
+
+            @pl.when(jnp.logical_not(relay))
+            def _():
+                Ps(n)[rows] = part.astype(BF16)
+
+            send(
+                Ps(n).at[rows], Rs(slot).at[rows], name, pre + (n, h),
+                dev(z + step, x, y, c), ridx=pre + (slot, h), keep=False,
+            )
 
     def line_total(A, pre, Rs, name):
         for cond, slot in ((below, z), (above, Z)):
 
             @pl.when(cond)
             def _():
-                recv(Rs(slot), name, pre + (slot,))
+                for h in range(H):
+                    recv(Rs(slot).at[h * TR // H : (h + 1) * TR // H], name, pre + (slot, h))
                 A[...] = A[...] + Rs(slot)[...].astype(F32)
 
     def kv_partial(zp):
@@ -351,6 +368,12 @@
     AKV[...] = kv_partial(z)
     q_steps = [(j, n) for j in range(J) for n in range(Z - 1)]
     q_step(*q_steps.pop(0))
+    def out_weight(j):
+        rows = slice(j * Gc, (j + 1) * Gc)
+        for d in range(1, X):
+            send(wo.at[rows], WOX.at[d - 1, rows], "wo", (d, j), xdev(d))
+
+    out_weight(0)
 
     low = lax.rem(lax.broadcasted_iota(jnp.int32, (TR, hd), 1), hd // 2) < hd // 4
 
@@ -374,14 +397,24 @@
         for e in range(1, X):
             send(KV.at[zp * X + x], KV.at[zp * X + x], "kx", (e, zp), xdev(e))
 
-    for n in range(Z - 1):
-        if q_steps:
-            q_step(*q_steps.pop(0))
+    edge = jnp.logical_or(z == 0, z == Z - 1)
+
+    def run_steps():
+        for step in q_steps:
+            q_step(*step)
+
+    pl.when(edge)(run_steps)
+
+    inner = jnp.logical_not(edge)
+    kv_hop(0)
+    kv_hop(1)
+    pl.when(inner)(lambda: q_step(*q_steps[0]))
+    for n in range(2, Z - 1):
         kv_hop(n)
-    for step in q_steps:
-        q_step(*step)
-    for d in range(1, X):
-        send(wo, WOX.at[d - 1], "wo", (d,), xdev(d))
+    for j in range(1, J):
+        out_weight(j)
+    for step in q_steps[1:]:
+        pl.when(inner)(lambda step=step: q_step(*step))
     for k in range(Z):
         for e in range(1, X):
             recv(KV.at[k * X + dn(x, e, X)], "kx", (e, k))
@@ -408,7 +441,8 @@
             send(AT.at[z, j], AT.at[z, j], "at", (j, up_down[0]), dev(up_down[1], x, y, c), ridx=(j, z), when=up_down[2])
 
     for d in range(1, X):
-        recv(WOX.at[d - 1], "wo", (d,))
+        for j in range(J):
+            recv(WOX.at[d - 1, j * Gc : (j + 1) * Gc], "wo", (d, j))
 
     def out_block(zp):
         for e in range(X):
@@ -467,11 +501,17 @@
     for k in range(Z):
         part = slice(k * X * No, (k + 1) * X * No)
         out[:, part] = (FB[k].astype(F32) * inv * og[:, part]).astype(BF16)
-    for make, when in sent:
+    for n in range(Z - 1):
+        for h in range(H):
+            rows = slice(h * TR // H, (h + 1) * TR // H)
+            sent.append((wait_for(PKV.at[n, rows], "pkv", (n, h)), None))
+            for j in range(J):
+                sent.append((wait_for(PQ.at[j, n, rows], "pq", (j, n, h)), None))
+    for wait, when in sent:
         if when is None:
-            make().wait_send()
+            wait()
         else:
-            pl.when(when)(lambda make=make: make().wait_send())
+            pl.when(when)(wait)
 
 
 def split_axis(n):

time: 166 us -> 152 us (0.916)
  Pallas kernels: 162 us -> 149 us
    pallas_call x1, Pallas kernels: 162 us -> 149 us  [fused_device(): pl.pallas_call(functools.partial(fused_kernel, *dims, names), out_shape=j...]
where the time goes in v3:
time: 152 us
  Pallas kernels  149 us (98%)
  local copies, waits for them, and re-layouts  1.87 us (1%)
    pallas_call x1, Pallas kernels, fused_device(): pl.pallas_call(functools.partial(fused_kernel, *dims, names), out_shape=j...  149 us

profile of v3, /device:TPU:0, one launch (start us, length us, event | category | flops | bytes accessed | tf_op | source)
XLA Modules:
  0.0 152.2 jit_solution(15737565052522087594)
XLA Ops:
  0.0 0.1 broadcast_multiply_fusion.1
  0.2 1.3 negate_select_fusion
  1.4 148.8 %shard_map.82 = bf16[64,4096]{1,0:T(8,128)(2,1)} custom-call(bf16[64,4096]{1,0:T(8,128)(2,1)} %refs_0_.1, bf16[512,1024]{1,0:T(8,128)(2,1)} %refs_1_.1, bf16[512,256]{1,0:T(8,128)(2,1)} %refs_2_.1, bf16[512,256]{1,0:T(8,128)(2,1)} %refs_3_.1, bf16[1024,512]{1,0:T(8,128)(2,1)} %refs_4_.1, f32[1,128]{1,0:T(1,128)} %bitcast.4, f32[1,128]{1,0:T(1,128)} %bitcast.5, ...), custom_call_target="tpu_custom_call" | custom-call | tf_op jit(solution)/shard_map/pallas_call | solution.py:578
  150.3 1.9 %copy.10 = bf16[64,4096]{1,0:T(8,128)(2,1)} copy(bf16[64,4096]{1,0:T(8,128)(2,1)} %shard_map.82) | data formatting | bytes 1048576
  (3 shorter events, 0.0 us)
